TPU v7x, 32 devices: a whole 2x2x4 slice. The times are simulated.
32 devices in a mesh: ep: 16 (over z, y, core), tp: 2 (over x).
Axes of the slice: x: 2, y: 2, z: 4, core: 2. Of those that a mesh axis runs over, the one named last changes fastest.
Arguments:
- tokens: bfloat16 [256, 2048], P('ep'), may hold values from -6 to 6
- recur_state: float32 [256, 8, 128, 128], P('ep', 'tp'), may hold values from -0.4 to 0.4
- attn_gain: float32 [2048], replicated, may hold values from 0.1 to 1.9
- query_weight: bfloat16 [2048, 1024], P(None, 'tp'), may hold values from -0.125 to 0.125
- key_weight: bfloat16 [2048, 1024], P(None, 'tp'), may hold values from -0.125 to 0.125
- value_weight: bfloat16 [2048, 1024], P(None, 'tp'), may hold values from -0.125 to 0.125
- outgate_weight: bfloat16 [2048, 1024], P(None, 'tp'), may hold values from -0.125 to 0.125
- beta_weight: bfloat16 [2048, 8], replicated, may hold values from -0.125 to 0.125
- decay_weight: bfloat16 [2048, 8], replicated, may hold values from -0.125 to 0.125
- decay_rate: float32 [8], replicated, may hold values from 0.05 to 2
- head_gain: float32 [128], replicated, may hold values from 0.1 to 1.9
- output_weight: bfloat16 [1024, 2048], P('tp'), may hold values from -0.1875 to 0.1875
- ffn_gain: float32 [2048], replicated, may hold values from 0.1 to 1.9
- routes: int32 [256, 2], P('ep'), may hold values from 0 to 3, all different within a row; in each aligned block of 16 rows (0 to 15, 16 to 31, ...) at most 16 rows name the same one
- route_weight: float32 [256, 2], P('ep'), may hold values from 0.2 to 1
- expert_gate: bfloat16 [16, 2048, 1024], P('ep', None, 'tp'), may hold values from -0.125 to 0.125
- expert_up: bfloat16 [16, 2048, 1024], P('ep', None, 'tp'), may hold values from -0.125 to 0.125
- expert_down: bfloat16 [16, 1024, 2048], P('ep', 'tp'), may hold values from -0.09375 to 0.09375
Outputs:
- mixed: bfloat16 [256, 2048], P('ep', 'tp')
- new_state: float32 [256, 8, 128, 128], P('ep', 'tp')
Inputs may be any that keep to these rules, and one draw needn't show every extreme that they name: `routes`: each row names 2 different experts; in each aligned block of 16 rows no expert is named by more than 16 rows.
All inputs are finite; a program needn't handle non-finite values.
Results may differ from a plain program's by a relative error of at most 0.014.
Values may be sent and summed in bfloat16 or wider, within the bound.
No kernel may reach another device: no remote copies, remote signals or barrier semaphores. Data moves between devices by JAX's collectives and lax.ppermute only.
A program may use at most 64 MiB of HBM per device.

v0:
```python
import functools

import jax
import jax.numpy as jnp
from jax import lax
from jax.experimental import pallas as pl
from jax.experimental.pallas import tpu as pltpu
from jax.sharding import Mesh, PartitionSpec as P


EPS = 1e-06
SLICES = 4
CORES = 2
FILL_FLOPS = 1 << 30
EP = ("outer", "mid", "core")
PLANE = ("mid", "tp")


def rms_scale(values, gain):
    return values * lax.rsqrt(jnp.mean(values * values, axis=-1, keepdims=True) + EPS) * gain


def unit_rows(values):
    return values * lax.rsqrt(jnp.sum(values * values, axis=-1, keepdims=True) + EPS)


def near(value):
    return pltpu.with_memory_space_constraint(value, pltpu.VMEM)


def far(value):
    return pltpu.with_memory_space_constraint(value, pltpu.HBM)


def swap(value, axes, offset):
    size = lax.axis_size(axes)
    return lax.ppermute(value, axes, [(i, i ^ offset) for i in range(size)])


def columns(value, index, width):
    return lax.dynamic_slice_in_dim(value, index * width, width, 1)


def split_two(value):
    high = value.astype(jnp.bfloat16)
    return [high, (value - high.astype(jnp.float32)).astype(jnp.bfloat16)]


def mixer_kernel(lanes, *refs):
    f32 = jnp.float32
    bf16 = jnp.bfloat16
    sources, refs = refs[:12], refs[12:]
    own_ref, sent_ref, key_ref, written_ref, fade_ref = refs[:5]
    targets, refs = refs[5:16], refs[16:]
    state_vmem, load_sem, state_sem = refs
    tokens_ref, gain_ref, beta_ref, decay_ref, rate_ref, head_gain_ref = targets[:6]
    _, _, _, _, output_vmem = targets[6:]
    rows, heads_here, head_size, _ = state_vmem.shape
    lane_index = lax.axis_index("tp")
    loads = [
        pltpu.make_async_copy(source, target, load_sem.at[place])
        for place, (source, target) in enumerate(zip(sources, targets))
    ]
    state_loads = [
        pltpu.make_async_copy(sources[11].at[:, head], state_vmem.at[:, head], state_sem.at[head])
        for head in range(heads_here)
    ]
    for copy in loads[:9] + state_loads + loads[9:]:
        copy.start()

    for copy in loads[:6]:
        copy.wait()
    normed = rms_scale(tokens_ref[...].astype(f32), gain_ref[...]).astype(bf16)
    across = (((1,), (1,)), ((), ()))
    strength = jax.nn.sigmoid(
        lax.dot_general(normed, beta_ref[...], across, preferred_element_type=f32)
    )
    softened = jax.nn.softplus(
        lax.dot_general(normed, decay_ref[...], across, preferred_element_type=f32)
    )
    fading = jnp.exp(-rate_ref[...] * softened)
    head_ids = lax.broadcasted_iota(jnp.int32, strength.shape, 1)

    def of_head(table, head):
        chosen = head_ids == lane_index * heads_here + head
        return jnp.sum(jnp.where(chosen, table, 0.0), axis=1, keepdims=True)

    def project(place):
        loads[place].wait()
        proj = jnp.dot(normed, targets[place][...], preferred_element_type=f32)
        return proj.astype(bf16).astype(f32)

    def lanes_of(head):
        return slice(head * head_size, (head + 1) * head_size)

    kproj = project(6)
    vproj = project(7)
    qproj = project(8)
    readouts = []
    for head in range(heads_here):
        keyvec = unit_rows(jax.nn.silu(kproj[:, lanes_of(head)]))
        query = unit_rows(jax.nn.silu(qproj[:, lanes_of(head)])) * head_size ** (-0.5)
        value = jax.nn.silu(vproj[:, lanes_of(head)])
        fade = of_head(fading, head)
        both = jnp.concatenate([keyvec, query], axis=0)
        left = jnp.concatenate(split_two(both), axis=0)
        left = jnp.concatenate([left, left], axis=1)
        row_ids = lax.rem(lax.broadcasted_iota(jnp.int32, both.shape, 0), rows)
        found = jnp.zeros(both.shape, f32)
        state_loads[head].wait()
        for row in range(0, rows, 2):
            block = jnp.concatenate([state_vmem[row, head], state_vmem[row + 1, head]], axis=1)
            right = jnp.concatenate(split_two(block), axis=0)
            seen = jnp.dot(left, right, preferred_element_type=f32)
            seen = seen[: 2 * rows] + seen[2 * rows :]
            found = jnp.where(row_ids == row, seen[:, :head_size], found)
            found = jnp.where(row_ids == row + 1, seen[:, head_size:], found)
        recall, asked = found[:rows], found[rows:]
        written = of_head(strength, head) * (value - fade * recall)
        overlap = jnp.sum(query * keyvec, axis=1, keepdims=True)
        readouts.append(fade * asked + overlap * written)
        key_ref[:, lanes_of(head)] = keyvec
        written_ref[:, lanes_of(head)] = written
        fade_ref[:, head : head + 1] = fade
    zproj = project(9)
    headed = jnp.concatenate(
        [
            (
                rms_scale(readouts[head], head_gain_ref[...])
                * jax.nn.silu(zproj[:, lanes_of(head)])
            ).astype(bf16)
            for head in range(heads_here)
        ],
        axis=1,
    )
    loads[10].wait()
    width = own_ref.shape[1]

    def part(position):
        start = pl.multiple_of(position * width, width)
        return jnp.dot(headed, output_vmem[:, pl.ds(start, width)], preferred_element_type=f32)

    for offset in range(1, lanes):
        sent_ref[(offset - 1) * rows : offset * rows, :] = part(lane_index ^ offset).astype(bf16)
    own_ref[...] = part(lane_index)


def mixer(
    tokens,
    recur_state,
    attn_gain,
    query_weight,
    key_weight,
    value_weight,
    outgate_weight,
    beta_weight,
    decay_weight,
    decay_rate,
    head_gain,
    output_weight,
):
    f32 = jnp.float32
    bf16 = jnp.bfloat16
    rows, model_width = tokens.shape
    heads_here, head_size = recur_state.shape[1:3]
    lanes = lax.axis_size("tp")
    width = model_width // lanes
    vmem = pl.BlockSpec(memory_space=pltpu.VMEM)
    hbm = pl.BlockSpec(memory_space=pltpu.HBM)
    inputs = (
        tokens,
        attn_gain[None],
        beta_weight.T,
        decay_weight.T,
        decay_rate[None],
        head_gain[None],
        key_weight,
        value_weight,
        query_weight,
        outgate_weight,
        output_weight,
    )
    return pl.pallas_call(
        functools.partial(mixer_kernel, lanes),
        out_shape=(
            pltpu.VMEM((rows, width), f32),
            pltpu.VMEM((rows * (lanes - 1), width), bf16),
            pltpu.VMEM((rows, heads_here * head_size), f32),
            pltpu.VMEM((rows, heads_here * head_size), f32),
            pltpu.VMEM((rows, heads_here), f32),
        ),
        in_specs=[hbm] * 12,
        out_specs=[vmem] * 5,
        scratch_shapes=[pltpu.VMEM(value.shape, value.dtype) for value in inputs]
        + [
            pltpu.VMEM(recur_state.shape, f32),
            pltpu.SemaphoreType.DMA((len(inputs),)),
            pltpu.SemaphoreType.DMA((heads_here,)),
        ],
        compiler_params=pltpu.CompilerParams(vmem_limit_bytes=20 << 20),
        name="mixer",
    )(*map(far, inputs + (recur_state,)))


def update_kernel(
    state_hbm, key_ref, written_ref, fade_ref, out_hbm, state_vmem, held, load_sem, sem
):
    rows, heads_here, head_size, _ = held.shape
    loads = [
        pltpu.make_async_copy(state_hbm.at[:, head], state_vmem.at[:, head], load_sem.at[head])
        for head in range(heads_here)
    ]
    copies = [
        pltpu.make_async_copy(held.at[:, head], out_hbm.at[:, head], sem.at[head])
        for head in range(heads_here)
    ]
    for copy in loads:
        copy.start()
    for head in range(heads_here):
        lanes = slice(head * head_size, (head + 1) * head_size)
        key_turned = key_ref[:, lanes].T
        written = written_ref[:, lanes]
        fade = fade_ref[:, head : head + 1]
        loads[head].wait()
        for row in range(rows):
            held[row, head] = (
                fade[row : row + 1, :] * state_vmem[row, head]
                + key_turned[:, row : row + 1] * written[row : row + 1, :]
            )
        copies[head].start()
    for copy in copies:
        copy.wait()


def update(state, keyvec, written, fade):
    vmem = pl.BlockSpec(memory_space=pltpu.VMEM)
    hbm = pl.BlockSpec(memory_space=pltpu.HBM)
    semaphores = pltpu.SemaphoreType.DMA((state.shape[1],))
    return pl.pallas_call(
        update_kernel,
        out_shape=pltpu.HBM(state.shape, state.dtype),
        in_specs=[hbm] + [vmem] * 3,
        out_specs=hbm,
        scratch_shapes=[pltpu.VMEM(state.shape, state.dtype)] * 2 + [semaphores] * 2,
        compiler_params=pltpu.CompilerParams(vmem_limit_bytes=12 << 20),
        cost_estimate=pl.CostEstimate(
            flops=FILL_FLOPS, transcendentals=0, bytes_accessed=8 * state.size
        ),
        name="update",
    )(far(state), *map(near, (keyvec, written, fade)))


def fetch_kernel(count, *refs):
    sources, targets, sem = refs[1 : 1 + count], refs[1 + count : 1 + 2 * count], refs[-1]
    copies = [
        pltpu.make_async_copy(source, target, sem.at[place])
        for place, (source, target) in enumerate(zip(sources, targets))
    ]
    for copy in copies:
        copy.start()
    for copy in copies:
        copy.wait()


def fetch(after, *arrays):
    vmem = pl.BlockSpec(memory_space=pltpu.VMEM)
    hbm = pl.BlockSpec(memory_space=pltpu.HBM)
    size = sum(value.size * value.dtype.itemsize for value in arrays)
    return pl.pallas_call(
        functools.partial(fetch_kernel, len(arrays)),
        out_shape=[pltpu.VMEM(value.shape, value.dtype) for value in arrays],
        in_specs=[vmem] + [hbm] * len(arrays),
        out_specs=[vmem] * len(arrays),
        scratch_shapes=[pltpu.SemaphoreType.DMA((len(arrays),))],
        compiler_params=pltpu.CompilerParams(vmem_limit_bytes=8 << 20),
        cost_estimate=pl.CostEstimate(
            flops=FILL_FLOPS, transcendentals=0, bytes_accessed=2 * size
        ),
        name="fetch",
    )(near(after), *map(far, arrays))


def expert_kernel(mid, lanes, *refs):
    f32 = jnp.float32
    bf16 = jnp.bfloat16
    pieces = mid * lanes
    arrived = refs[: CORES * pieces]
    gain_ref, gate_ref, up_ref, down_ref = refs[CORES * pieces : CORES * pieces + 4]
    outs = refs[CORES * pieces + 4 : CORES * pieces + 4 + CORES * pieces]
    ffn_vmem = refs[CORES * pieces + 4 + CORES * pieces]
    band = arrived[0].shape[0]
    model_width = ffn_vmem.shape[1]
    width = model_width // lanes
    lane_index = lax.axis_index("tp")

    def columns_of(offset):
        return pl.ds(pl.multiple_of((lane_index ^ offset) * width, width), width)

    for block in range(CORES * mid):
        rows = slice(block * band, (block + 1) * band)
        parts = arrived[block * lanes : (block + 1) * lanes]
        squares = 0.0
        for part in parts:
            value = part[...].astype(f32)
            squares = squares + jnp.sum(value * value, axis=-1, keepdims=True)
        scale = lax.rsqrt(squares / model_width + EPS)
        for offset, part in enumerate(parts):
            where = columns_of(offset)
            ffn_vmem[rows, where] = (part[...].astype(f32) * scale * gain_ref[:, where]).astype(
                bf16
            )
    ffn_in = ffn_vmem[...]
    gated = jnp.dot(ffn_in, gate_ref[0], preferred_element_type=f32)
    lifted = jnp.dot(ffn_in, up_ref[0], preferred_element_type=f32)
    hidden = (jax.nn.silu(gated) * lifted).astype(bf16)
    for offset in range(lanes):
        terms = jnp.dot(hidden, down_ref[0, :, columns_of(offset)], preferred_element_type=f32)
        for block in range(CORES * mid):
            out = outs[block * lanes + offset]
            out[...] = terms[block * band : (block + 1) * band].astype(out.dtype)


def expert_slice(arrived, ffn_gain, expert_gate, expert_up, expert_down):
    f32 = jnp.float32
    bf16 = jnp.bfloat16
    mid, lanes = lax.axis_size("mid"), lax.axis_size("tp")
    model_width = ffn_gain.shape[0]
    band = arrived[0].shape[0]
    vmem = pl.BlockSpec(memory_space=pltpu.VMEM)
    shape = (band, model_width // lanes)
    rows = CORES * mid * band
    return pl.pallas_call(
        functools.partial(expert_kernel, mid, lanes),
        out_shape=[pltpu.VMEM(shape, f32)] * (mid * lanes)
        + [pltpu.VMEM(shape, bf16)] * (mid * lanes),
        in_specs=[vmem] * (CORES * mid * lanes + 4),
        out_specs=[vmem] * (CORES * mid * lanes),
        scratch_shapes=[pltpu.VMEM((rows, model_width), bf16)],
        compiler_params=pltpu.CompilerParams(vmem_limit_bytes=24 << 20),
        name="experts",
    )(*map(near, (*arrived, ffn_gain[None], expert_gate, expert_up, expert_down)))


def local(
    tokens,
    recur_state,
    attn_gain,
    query_weight,
    key_weight,
    value_weight,
    outgate_weight,
    beta_weight,
    decay_weight,
    decay_rate,
    head_gain,
    output_weight,
    ffn_gain,
    routes,
    route_weight,
    expert_gate,
    expert_up,
    expert_down,
):
    f32 = jnp.float32
    bf16 = jnp.bfloat16
    rows, model_width = tokens.shape
    outer = lax.axis_size("outer")
    mid = lax.axis_size("mid")
    lanes = lax.axis_size("tp")
    lane_index = lax.axis_index("tp")
    expert_index = lax.axis_index("outer")
    width = model_width // lanes

    branch, sent, *memory = mixer(
        tokens,
        recur_state,
        attn_gain,
        query_weight,
        key_weight,
        value_weight,
        outgate_weight,
        beta_weight,
        decay_weight,
        decay_rate,
        head_gain,
        output_weight,
    )
    for offset in range(1, lanes):
        piece = sent[(offset - 1) * rows : offset * rows]
        branch = branch + swap(piece, "tp", offset).astype(f32)
    resid = (
        columns(tokens, lane_index, width).astype(f32) + branch.astype(bf16).astype(f32)
    ).astype(bf16)

    new_state = update(recur_state, *memory)

    def weight_of(offset):
        named = routes == expert_index ^ offset
        return jnp.sum(jnp.where(named, route_weight, 0.0), axis=1, keepdims=True)

    held = resid
    held = jnp.concatenate(
        [held] + [swap(held, "outer", offset) for offset in range(1, outer)], axis=0
    )
    arrived = [held] + [swap(held, PLANE, offset) for offset in range(1, mid * lanes)]
    arrived = arrived + [swap(piece, "core", 1) for piece in arrived]
    fetched = fetch(sent, expert_gate, expert_up, expert_down)
    terms = expert_slice(arrived, ffn_gain, *fetched)
    own, other = terms[: mid * lanes], terms[mid * lanes :]
    total = own[0] + swap(other[0], "core", 1).astype(f32)
    for offset in range(1, mid * lanes):
        piece = (own[offset] + swap(other[offset], "core", 1).astype(f32)).astype(bf16)
        total = total + swap(piece, PLANE, offset).astype(f32)
    pieces = total.astype(bf16)
    moe = total[:rows] * weight_of(0)
    for offset in range(1, outer):
        piece = swap(pieces[offset * rows : (offset + 1) * rows], "outer", offset)
        moe = moe + piece.astype(f32) * weight_of(offset)
    mixed = (resid.astype(f32) + moe).astype(bf16)
    return (mixed, new_state)


def solution(mesh):
    groups, lanes = mesh.shape["ep"], mesh.shape["tp"]
    shape = (groups // SLICES, SLICES // CORES, CORES, lanes)
    inner = Mesh(mesh.devices.reshape(shape), EP + ("tp",))
    return jax.shard_map(
        local,
        mesh=inner,
        in_specs=(
            P(EP, None),
            P(EP, "tp", None, None),
            P(),
            P(None, "tp"),
            P(None, "tp"),
            P(None, "tp"),
            P(None, "tp"),
            P(),
            P(),
            P(),
            P(),
            P("tp", None),
            P(),
            P(EP, None),
            P(EP, None),
            P(EP, None, "tp"),
            P(EP, None, "tp"),
            P(EP, "tp", None),
        ),
        out_specs=(P(EP, "tp"), P(EP, "tp", None, None)),
        check_vma=False,
    )
```

profile of v0, /device:TPU:0, one launch (start us, length us, event | category | flops | bytes accessed | tf_op | source)
XLA Modules:
  0.0 56.4 jit_solution(13154911507745809794)
XLA Ops:
  0.6 6.0 %mixer.1 = (f32[16,1024]{1,0:T(8,128)S(1)}, bf16[16,1024]{1,0:T(8,128)(2,1)S(1)}, f32[16,512]{1,0:T(8,128)S(1)}, f32[16,512]{1,0:T(8,128)S(1)}, f32[16,4]{1,0:T(8,128)S(1)}) custom-call(bf16[16,2048]{1,0:T(8,128)(2,1)} %refs_0_.1, f32[1,2048]{1,0:T(1,128)} %bitcast.9, bf16[8,2048]{1,0:T(8,128)(2,1)} %bitcast.7, bf16[8,2048]{1,0:T(8,128)(2,1)} %bitcast.8, ...), custom_call_target="tpu_custom_call" | custom-call | tf_op jit(solution)/shard_map/mixer/pallas_call | solution.py:183
  6.6 3.0 %collective-permute-start = (bf16[16,1024]{1,0:T(8,128)(2,1)S(1)}, bf16[16,1024]{1,0:T(8,128)(2,1)S(1)}, u32[]{:S(2)}, u32[]{:S(2)}) collective-permute-start(bf16[16,1024]{1,0:T(8,128)(2,1)S(1)} %get-tuple-element.19.refs_0_), channel_id=1, source_target_pairs={{0,1},{1,0},{2,3},{3,2},{4,5},{5,4},{6,7},{7,6},{8,9},{9,8},{10,11... | collective-permute-start | bytes 98312 | tf_op jit(solution)/shard_map/ppermute | solution.py:37
  9.7 1.9 %collective-permute-done = bf16[16,1024]{1,0:T(8,128)(2,1)S(1)} collective-permute-done((bf16[16,1024]{1,0:T(8,128)(2,1)S(1)}, bf16[16,1024]{1,0:T(8,128)(2,1)S(1)}, u32[]{:S(2)}, u32[]{:S(2)}) %collective-permute-start) | collective-permute-done | bytes 32800 | tf_op jit(solution)/shard_map/ppermute | solution.py:37
  11.6 2.2 %collective-permute-start.1 = (bf16[16,1024]{1,0:T(8,128)(2,1)S(1)}, bf16[16,1024]{1,0:T(8,128)(2,1)S(1)}, u32[]{:S(2)}, u32[]{:S(2)}) collective-permute-start(bf16[16,1024]{1,0:T(8,128)(2,1)S(1)} %add_convert_fusion.3), channel_id=1, source_target_pairs={{0,8},{8,0},{16,24},{24,16},{1,9},{9,1},{17,25},{25,17},{2,10},{10... | collective-permute-start | bytes 98312 | tf_op jit(solution)/shard_map/ppermute | solution.py:37
  13.7 2.6 %collective-permute-start.2 = (bf16[16,1024]{1,0:T(8,128)(2,1)S(1)}, bf16[16,1024]{1,0:T(8,128)(2,1)S(1)}, u32[]{:S(2)}, u32[]{:S(2)}) collective-permute-start(bf16[16,1024]{1,0:T(8,128)(2,1)S(1)} %add_convert_fusion.3), channel_id=1, source_target_pairs={{0,16},{8,24},{16,0},{24,8},{1,17},{9,25},{17,1},{25,9},{2,18},{10... | collective-permute-start | bytes 98312 | tf_op jit(solution)/shard_map/ppermute | solution.py:37
  16.3 0.0 collective-permute-start.3
  16.3 0.0 collective-permute-done.1
  16.3 2.5 %collective-permute-done.2 = bf16[16,1024]{1,0:T(8,128)(2,1)S(1)} collective-permute-done((bf16[16,1024]{1,0:T(8,128)(2,1)S(1)}, bf16[16,1024]{1,0:T(8,128)(2,1)S(1)}, u32[]{:S(2)}, u32[]{:S(2)}) %collective-permute-start.2) | collective-permute-done | bytes 32800 | tf_op jit(solution)/shard_map/ppermute | solution.py:37
  18.8 3.2 %collective-permute-done.3 = bf16[16,1024]{1,0:T(8,128)(2,1)S(1)} collective-permute-done((bf16[16,1024]{1,0:T(8,128)(2,1)S(1)}, bf16[16,1024]{1,0:T(8,128)(2,1)S(1)}, u32[]{:S(2)}, u32[]{:S(2)}) %collective-permute-start.3) | collective-permute-done | bytes 32800 | tf_op jit(solution)/shard_map/ppermute | solution.py:37
  22.1 0.0 copy-start
  22.1 2.5 %collective-permute-start.6 = (bf16[64,1024]{1,0:T(8,128)(2,1)S(1)}, bf16[64,1024]{1,0:T(8,128)(2,1)S(1)}, u32[]{:S(2)}, u32[]{:S(2)}) collective-permute-start(bf16[64,1024]{1,0:T(8,128)(2,1)S(1)} %pad_maximum_fusion.refs_0_), channel_id=1, source_target_pairs={{0,5},{1,4},{4,1},{5,0},{2,7},{3,6},{6,3},{7,2},{8,13},{9,12},{12,... | collective-permute-start | bytes 393224 | tf_op jit(solution)/shard_map/ppermute | solution.py:37
  24.6 0.5 collective-permute-start.4
  25.1 0.5 collective-permute-start.5
  25.6 0.0 collective-permute-start.7
  25.6 2.4 %collective-permute-done.6.refs_3_ = bf16[64,1024]{1,0:T(8,128)(2,1)S(1)} collective-permute-done((bf16[64,1024]{1,0:T(8,128)(2,1)S(1)}, bf16[64,1024]{1,0:T(8,128)(2,1)S(1)}, u32[]{:S(2)}, u32[]{:S(2)}) %collective-permute-start.6) | collective-permute-done | bytes 131104 | tf_op jit(solution)/shard_map/ppermute | solution.py:37
  28.0 0.0 collective-permute-start.10
  28.0 1.5 %collective-permute-done.4.refs_1_ = bf16[64,1024]{1,0:T(8,128)(2,1)S(1)} collective-permute-done((bf16[64,1024]{1,0:T(8,128)(2,1)S(1)}, bf16[64,1024]{1,0:T(8,128)(2,1)S(1)}, u32[]{:S(2)}, u32[]{:S(2)}) %collective-permute-start.4) | collective-permute-done | bytes 131104 | tf_op jit(solution)/shard_map/ppermute | solution.py:37
  29.6 0.0 collective-permute-start.8
  29.6 0.5 collective-permute-done.5.refs_2_
  30.1 0.0 collective-permute-start.9
  30.1 2.9 %fetch.1 = (bf16[1,2048,512]{2,1,0:T(8,128)(2,1)S(1)}, bf16[1,2048,512]{2,1,0:T(8,128)(2,1)S(1)}, bf16[1,512,2048]{2,1,0:T(8,128)(2,1)S(1)}) custom-call(bf16[16,1024]{1,0:T(8,128)(2,1)S(1)} %get-tuple-element.19.refs_0_, bf16[1,2048,512]{2,1,0:T(8,128)(2,1)} %refs_1_.1, bf16[1,2048,512]{2,1,0:T(8,128)(2,1)} %refs_2_.1, bf16[1,512,2048]{2,1,0:T(8,128)(2,1)} %refs_3_.1), custom_call_target="tpu_custom_call" | custom-call | flops 1073741824 | bytes 12582912 | tf_op jit(solution)/shard_map/fetch/pallas_call | solution.py:269
  33.0 0.0 collective-permute-done.7.refs_4_
  33.0 0.0 collective-permute-done.10.refs_7_
  33.0 0.0 collective-permute-done.8.refs_5_
  33.0 0.0 collective-permute-done.9.refs_6_
  33.0 0.0 copy-start.2
  33.1 0.0 copy-start.3
  33.1 2.3 %experts.1 = (f32[64,1024]{1,0:T(8,128)S(1)}, f32[64,1024]{1,0:T(8,128)S(1)}, f32[64,1024]{1,0:T(8,128)S(1)}, f32[64,1024]{1,0:T(8,128)S(1)}, bf16[64,1024]{1,0:...) custom-call(bf16[64,1024]{1,0:T(8,128)(2,1)S(1)} %pad_maximum_fusion.ref, ...), custom_call_target="tpu_custom_call" | custom-call | tf_op jit(solution)/shard_map/experts/pallas_call | solution.py:332
  35.4 0.6 %collective-permute-start.12 = (bf16[64,1024]{1,0:T(8,128)(2,1)S(1)}, bf16[64,1024]{1,0:T(8,128)(2,1)S(1)}, u32[]{:S(2)}, u32[]{:S(2)}) collective-permute-start(bf16[64,1024]{1,0:T(8,128)(2,1)S(1)} %get-tuple-element.26), channel_id=1, source_target_pairs={{0,2},{2,0},{1,3},{3,1},{4,6},{6,4},{5,7},{7,5},{8,10},{10,8},{9,1... | collective-permute-start | bytes 393224 | tf_op jit(solution)/shard_map/ppermute | solution.py:37
  36.0 0.1 collective-permute-start.14
  36.1 0.4 collective-permute-start.16
  36.5 0.1 collective-permute-start.11
  36.6 0.4 collective-permute-done.12
  37.0 1.6 %collective-permute-start.13 = (bf16[64,1024]{1,0:T(8,128)(2,1)S(1)}, bf16[64,1024]{1,0:T(8,128)(2,1)S(1)}, u32[]{:S(2)}, u32[]{:S(2)}) collective-permute-start(bf16[64,1024]{1,0:T(8,128)(2,1)S(1)} %add_convert_fusion.2), channel_id=1, source_target_pairs={{0,1},{1,0},{4,5},{5,4},{2,3},{3,2},{6,7},{7,6},{8,9},{9,8},{12,13... | collective-permute-start | bytes 393224 | tf_op jit(solution)/shard_map/ppermute | solution.py:37
  38.6 0.0 collective-permute-done.14
  38.6 0.9 %collective-permute-start.15 = (bf16[64,1024]{1,0:T(8,128)(2,1)S(1)}, bf16[64,1024]{1,0:T(8,128)(2,1)S(1)}, u32[]{:S(2)}, u32[]{:S(2)}) collective-permute-start(bf16[64,1024]{1,0:T(8,128)(2,1)S(1)} %add_convert_fusion.1), channel_id=1, source_target_pairs={{0,4},{1,5},{4,0},{5,1},{2,6},{3,7},{6,2},{7,3},{8,12},{9,13},{12,... | collective-permute-start | bytes 393224 | tf_op jit(solution)/shard_map/ppermute | solution.py:37
  39.5 0.0 collective-permute-done.16
  39.5 1.2 %collective-permute-start.17 = (bf16[64,1024]{1,0:T(8,128)(2,1)S(1)}, bf16[64,1024]{1,0:T(8,128)(2,1)S(1)}, u32[]{:S(2)}, u32[]{:S(2)}) collective-permute-start(bf16[64,1024]{1,0:T(8,128)(2,1)S(1)} %add_convert_fusion), channel_id=1, source_target_pairs={{0,5},{1,4},{4,1},{5,0},{2,7},{3,6},{6,3},{7,2},{8,13},{9,12},{12,... | collective-permute-start | bytes 393224 | tf_op jit(solution)/shard_map/ppermute | solution.py:37
  40.8 2.3 %collective-permute-done.13 = bf16[64,1024]{1,0:T(8,128)(2,1)S(1)} collective-permute-done((bf16[64,1024]{1,0:T(8,128)(2,1)S(1)}, bf16[64,1024]{1,0:T(8,128)(2,1)S(1)}, u32[]{:S(2)}, u32[]{:S(2)}) %collective-permute-start.13) | collective-permute-done | bytes 131104 | tf_op jit(solution)/shard_map/ppermute | solution.py:37
  43.0 3.9 %collective-permute-done.15 = bf16[64,1024]{1,0:T(8,128)(2,1)S(1)} collective-permute-done((bf16[64,1024]{1,0:T(8,128)(2,1)S(1)}, bf16[64,1024]{1,0:T(8,128)(2,1)S(1)}, u32[]{:S(2)}, u32[]{:S(2)}) %collective-permute-start.15) | collective-permute-done | bytes 131104 | tf_op jit(solution)/shard_map/ppermute | solution.py:37
  46.9 0.0 collective-permute-done.17
  46.9 0.1 fusion.9
  47.1 0.1 collective-permute-start.18
  47.1 0.9 %collective-permute-start.19 = (bf16[16,1024]{1,0:T(8,128)(2,1)S(1)}, bf16[16,1024]{1,0:T(8,128)(2,1)S(1)}, u32[]{:S(2)}, u32[]{:S(2)}) collective-permute-start(bf16[16,1024]{1,0:T(8,128)(2,1)S(1)} %get-tuple-element.42), channel_id=1, source_target_pairs={{0,16},{8,24},{16,0},{24,8},{1,17},{9,25},{17,1},{25,9},{2,18},{10... | collective-permute-start | bytes 98312 | tf_op jit(solution)/shard_map/ppermute | solution.py:37
  48.0 3.5 %collective-permute-start.20 = (bf16[16,1024]{1,0:T(8,128)(2,1)S(1)}, bf16[16,1024]{1,0:T(8,128)(2,1)S(1)}, u32[]{:S(2)}, u32[]{:S(2)}) collective-permute-start(bf16[16,1024]{1,0:T(8,128)(2,1)S(1)} %get-tuple-element.41), channel_id=1, source_target_pairs={{0,24},{8,16},{16,8},{24,0},{1,25},{9,17},{17,9},{25,1},{2,26},{10... | collective-permute-start | bytes 98312 | tf_op jit(solution)/shard_map/ppermute | solution.py:37
  51.5 4.1 %update.1 = f32[16,4,128,128]{3,2,1,0:T(8,128)} custom-call(f32[16,4,128,128]{3,2,1,0:T(8,128)} %state_hbm.1, f32[16,512]{1,0:T(8,128)S(1)} %get-tuple-element.31.key_ref, f32[16,512]{1,0:T(8,128)S(1)} %get-tuple-element.32.written_ref, f32[16,4]{1,0:T(8,128)S(1)} %get-tuple-element.33.fade_ref), custom_call_target="tpu_custom_call" | custom-call | flops 1073741824 | bytes 8388608 | tf_op jit(solution)/shard_map/update/pallas_call | solution.py:239
  55.6 0.0 collective-permute-done.19
  55.6 0.7 %fusion.4 = bf16[16,1024]{1,0:T(8,128)(2,1)} fusion(f32[64,1024]{1,0:T(8,128)S(1)} %get-tuple-element.39, bf16[16,1024]{1,0:T(8,128)(2,1)S(1)} %collective-permute-done.20, bf16[16,1024]{1,0:T(8,128)(2,1)S(1)} %collective-permute-done.19, bf16[16,1024]{1,0:T(8,128)(2,1)S(1)} %collective-permute-done.18, bf16[16,1024]{1,0:T(8,128)(2,1)S(1)} %add_convert_fusion.3, ...), kind=kLoop, calls=%fused_computation.10 | loop fusion | flops 212992 | bytes 229632 | tf_op jit(solution)/shard_map/convert_element_type | solution.py:419
  (15 shorter events, 0.2 us)
Async XLA Ops:
  0.6 10.9 %copy-start.1 = (bf16[16,2048]{1,0:T(8,128)(2,1)S(1)}, bf16[16,2048]{1,0:T(8,128)(2,1)}, u32[]{:S(2)}) copy-start(bf16[16,2048]{1,0:T(8,128)(2,1)} %refs_0_.1) | copy-start | bytes 196612
  6.6 4.9 %collective-permute-start = (bf16[16,1024]{1,0:T(8,128)(2,1)S(1)}, bf16[16,1024]{1,0:T(8,128)(2,1)S(1)}, u32[]{:S(2)}, u32[]{:S(2)}) collective-permute-start(bf16[16,1024]{1,0:T(8,128)(2,1)S(1)} %get-tuple-element.19.refs_0_), channel_id=1, source_target_pairs={{0,1},{1,0},{2,3},{3,2},{4,5},{5,4},{6,7},{7,6},{8,9},{9,8},{10,11... | collective-permute-start | bytes 98312 | tf_op jit(solution)/shard_map/ppermute | solution.py:37
  11.6 4.8 %collective-permute-start.1 = (bf16[16,1024]{1,0:T(8,128)(2,1)S(1)}, bf16[16,1024]{1,0:T(8,128)(2,1)S(1)}, u32[]{:S(2)}, u32[]{:S(2)}) collective-permute-start(bf16[16,1024]{1,0:T(8,128)(2,1)S(1)} %add_convert_fusion.3), channel_id=1, source_target_pairs={{0,8},{8,0},{16,24},{24,16},{1,9},{9,1},{17,25},{25,17},{2,10},{10... | collective-permute-start | bytes 98312 | tf_op jit(solution)/shard_map/ppermute | solution.py:37
  13.7 5.1 %collective-permute-start.2 = (bf16[16,1024]{1,0:T(8,128)(2,1)S(1)}, bf16[16,1024]{1,0:T(8,128)(2,1)S(1)}, u32[]{:S(2)}, u32[]{:S(2)}) collective-permute-start(bf16[16,1024]{1,0:T(8,128)(2,1)S(1)} %add_convert_fusion.3), channel_id=1, source_target_pairs={{0,16},{8,24},{16,0},{24,8},{1,17},{9,25},{17,1},{25,9},{2,18},{10... | collective-permute-start | bytes 98312 | tf_op jit(solution)/shard_map/ppermute | solution.py:37
  16.3 5.7 %collective-permute-start.3 = (bf16[16,1024]{1,0:T(8,128)(2,1)S(1)}, bf16[16,1024]{1,0:T(8,128)(2,1)S(1)}, u32[]{:S(2)}, u32[]{:S(2)}) collective-permute-start(bf16[16,1024]{1,0:T(8,128)(2,1)S(1)} %add_convert_fusion.3), channel_id=1, source_target_pairs={{0,24},{8,16},{16,8},{24,0},{1,25},{9,17},{17,9},{25,1},{2,26},{10... | collective-permute-start | bytes 98312 | tf_op jit(solution)/shard_map/ppermute | solution.py:37
  22.1 11.0 %copy-start = (f32[2048]{0:T(1024)S(1)}, f32[2048]{0:T(1024)}, u32[]{:S(2)}) copy-start(f32[2048]{0:T(1024)} %param.30) | copy-start | bytes 24580
  22.1 5.9 %collective-permute-start.6 = (bf16[64,1024]{1,0:T(8,128)(2,1)S(1)}, bf16[64,1024]{1,0:T(8,128)(2,1)S(1)}, u32[]{:S(2)}, u32[]{:S(2)}) collective-permute-start(bf16[64,1024]{1,0:T(8,128)(2,1)S(1)} %pad_maximum_fusion.refs_0_), channel_id=1, source_target_pairs={{0,5},{1,4},{4,1},{5,0},{2,7},{3,6},{6,3},{7,2},{8,13},{9,12},{12,... | collective-permute-start | bytes 393224 | tf_op jit(solution)/shard_map/ppermute | solution.py:37
  24.6 5.0 %collective-permute-start.4 = (bf16[64,1024]{1,0:T(8,128)(2,1)S(1)}, bf16[64,1024]{1,0:T(8,128)(2,1)S(1)}, u32[]{:S(2)}, u32[]{:S(2)}) collective-permute-start(bf16[64,1024]{1,0:T(8,128)(2,1)S(1)} %pad_maximum_fusion.refs_0_), channel_id=1, source_target_pairs={{0,1},{1,0},{4,5},{5,4},{2,3},{3,2},{6,7},{7,6},{8,9},{9,8},{12,13... | collective-permute-start | bytes 393224 | tf_op jit(solution)/shard_map/ppermute | solution.py:37
  25.1 5.0 %collective-permute-start.5 = (bf16[64,1024]{1,0:T(8,128)(2,1)S(1)}, bf16[64,1024]{1,0:T(8,128)(2,1)S(1)}, u32[]{:S(2)}, u32[]{:S(2)}) collective-permute-start(bf16[64,1024]{1,0:T(8,128)(2,1)S(1)} %pad_maximum_fusion.refs_0_), channel_id=1, source_target_pairs={{0,4},{1,5},{4,0},{5,1},{2,6},{3,7},{6,2},{7,3},{8,12},{9,13},{12,... | collective-permute-start | bytes 393224 | tf_op jit(solution)/shard_map/ppermute | solution.py:37
  25.6 7.4 %collective-permute-start.7 = (bf16[64,1024]{1,0:T(8,128)(2,1)S(1)}, bf16[64,1024]{1,0:T(8,128)(2,1)S(1)}, u32[]{:S(2)}, u32[]{:S(2)}) collective-permute-start(bf16[64,1024]{1,0:T(8,128)(2,1)S(1)} %pad_maximum_fusion.refs_0_), channel_id=1, source_target_pairs={{0,2},{2,0},{1,3},{3,1},{4,6},{6,4},{5,7},{7,5},{8,10},{10,8},{9,1... | collective-permute-start | bytes 393224 | tf_op jit(solution)/shard_map/ppermute | solution.py:37
  28.0 5.0 %collective-permute-start.10 = (bf16[64,1024]{1,0:T(8,128)(2,1)S(1)}, bf16[64,1024]{1,0:T(8,128)(2,1)S(1)}, u32[]{:S(2)}, u32[]{:S(2)}) collective-permute-start(bf16[64,1024]{1,0:T(8,128)(2,1)S(1)} %collective-permute-done.6.refs_3_), channel_id=1, source_target_pairs={{0,2},{2,0},{1,3},{3,1},{4,6},{6,4},{5,7},{7,5},{8,10},{10,8},{9,1... | collective-permute-start | bytes 393224 | tf_op jit(solution)/shard_map/ppermute | solution.py:37
  29.6 3.5 %collective-permute-start.8 = (bf16[64,1024]{1,0:T(8,128)(2,1)S(1)}, bf16[64,1024]{1,0:T(8,128)(2,1)S(1)}, u32[]{:S(2)}, u32[]{:S(2)}) collective-permute-start(bf16[64,1024]{1,0:T(8,128)(2,1)S(1)} %collective-permute-done.4.refs_1_), channel_id=1, source_target_pairs={{0,2},{2,0},{1,3},{3,1},{4,6},{6,4},{5,7},{7,5},{8,10},{10,8},{9,1... | collective-permute-start | bytes 393224 | tf_op jit(solution)/shard_map/ppermute | solution.py:37
  30.1 2.9 %collective-permute-start.9 = (bf16[64,1024]{1,0:T(8,128)(2,1)S(1)}, bf16[64,1024]{1,0:T(8,128)(2,1)S(1)}, u32[]{:S(2)}, u32[]{:S(2)}) collective-permute-start(bf16[64,1024]{1,0:T(8,128)(2,1)S(1)} %collective-permute-done.5.refs_2_), channel_id=1, source_target_pairs={{0,2},{2,0},{1,3},{3,1},{4,6},{6,4},{5,7},{7,5},{8,10},{10,8},{9,1... | collective-permute-start | bytes 393224 | tf_op jit(solution)/shard_map/ppermute | solution.py:37
  33.0 7.7 %copy-start.2 = (f32[16,2]{0,1:T(2,128)S(1)}, f32[16,2]{0,1:T(2,128)}, u32[]{:S(2)}) copy-start(f32[16,2]{0,1:T(2,128)} %param.32) | copy-start | bytes 388
  33.1 7.7 %copy-start.3 = (s32[16,2]{0,1:T(2,128)S(1)}, s32[16,2]{0,1:T(2,128)}, u32[]{:S(2)}) copy-start(s32[16,2]{0,1:T(2,128)} %param.31) | copy-start | bytes 388
  35.4 1.6 %collective-permute-start.12 = (bf16[64,1024]{1,0:T(8,128)(2,1)S(1)}, bf16[64,1024]{1,0:T(8,128)(2,1)S(1)}, u32[]{:S(2)}, u32[]{:S(2)}) collective-permute-start(bf16[64,1024]{1,0:T(8,128)(2,1)S(1)} %get-tuple-element.26), channel_id=1, source_target_pairs={{0,2},{2,0},{1,3},{3,1},{4,6},{6,4},{5,7},{7,5},{8,10},{10,8},{9,1... | collective-permute-start | bytes 393224 | tf_op jit(solution)/shard_map/ppermute | solution.py:37
  36.0 2.6 %collective-permute-start.14 = (bf16[64,1024]{1,0:T(8,128)(2,1)S(1)}, bf16[64,1024]{1,0:T(8,128)(2,1)S(1)}, u32[]{:S(2)}, u32[]{:S(2)}) collective-permute-start(bf16[64,1024]{1,0:T(8,128)(2,1)S(1)} %get-tuple-element.28), channel_id=1, source_target_pairs={{0,2},{2,0},{1,3},{3,1},{4,6},{6,4},{5,7},{7,5},{8,10},{10,8},{9,1... | collective-permute-start | bytes 393224 | tf_op jit(solution)/shard_map/ppermute | solution.py:37
  36.1 3.4 %collective-permute-start.16 = (bf16[64,1024]{1,0:T(8,128)(2,1)S(1)}, bf16[64,1024]{1,0:T(8,128)(2,1)S(1)}, u32[]{:S(2)}, u32[]{:S(2)}) collective-permute-start(bf16[64,1024]{1,0:T(8,128)(2,1)S(1)} %get-tuple-element.30), channel_id=1, source_target_pairs={{0,2},{2,0},{1,3},{3,1},{4,6},{6,4},{5,7},{7,5},{8,10},{10,8},{9,1... | collective-permute-start | bytes 393224 | tf_op jit(solution)/shard_map/ppermute | solution.py:37
  36.5 4.3 %collective-permute-start.11 = (bf16[64,1024]{1,0:T(8,128)(2,1)S(1)}, bf16[64,1024]{1,0:T(8,128)(2,1)S(1)}, u32[]{:S(2)}, u32[]{:S(2)}) collective-permute-start(bf16[64,1024]{1,0:T(8,128)(2,1)S(1)} %get-tuple-element.24), channel_id=1, source_target_pairs={{0,2},{2,0},{1,3},{3,1},{4,6},{6,4},{5,7},{7,5},{8,10},{10,8},{9,1... | collective-permute-start | bytes 393224 | tf_op jit(solution)/shard_map/ppermute | solution.py:37
  37.0 6.0 %collective-permute-start.13 = (bf16[64,1024]{1,0:T(8,128)(2,1)S(1)}, bf16[64,1024]{1,0:T(8,128)(2,1)S(1)}, u32[]{:S(2)}, u32[]{:S(2)}) collective-permute-start(bf16[64,1024]{1,0:T(8,128)(2,1)S(1)} %add_convert_fusion.2), channel_id=1, source_target_pairs={{0,1},{1,0},{4,5},{5,4},{2,3},{3,2},{6,7},{7,6},{8,9},{9,8},{12,13... | collective-permute-start | bytes 393224 | tf_op jit(solution)/shard_map/ppermute | solution.py:37
  38.6 8.4 %collective-permute-start.15 = (bf16[64,1024]{1,0:T(8,128)(2,1)S(1)}, bf16[64,1024]{1,0:T(8,128)(2,1)S(1)}, u32[]{:S(2)}, u32[]{:S(2)}) collective-permute-start(bf16[64,1024]{1,0:T(8,128)(2,1)S(1)} %add_convert_fusion.1), channel_id=1, source_target_pairs={{0,4},{1,5},{4,0},{5,1},{2,6},{3,7},{6,2},{7,3},{8,12},{9,13},{12,... | collective-permute-start | bytes 393224 | tf_op jit(solution)/shard_map/ppermute | solution.py:37
  39.5 7.4 %collective-permute-start.17 = (bf16[64,1024]{1,0:T(8,128)(2,1)S(1)}, bf16[64,1024]{1,0:T(8,128)(2,1)S(1)}, u32[]{:S(2)}, u32[]{:S(2)}) collective-permute-start(bf16[64,1024]{1,0:T(8,128)(2,1)S(1)} %add_convert_fusion), channel_id=1, source_target_pairs={{0,5},{1,4},{4,1},{5,0},{2,7},{3,6},{6,3},{7,2},{8,13},{9,12},{12,... | collective-permute-start | bytes 393224 | tf_op jit(solution)/shard_map/ppermute | solution.py:37
  47.1 8.6 %collective-permute-start.18 = (bf16[16,1024]{1,0:T(8,128)(2,1)S(1)}, bf16[16,1024]{1,0:T(8,128)(2,1)S(1)}, u32[]{:S(2)}, u32[]{:S(2)}) collective-permute-start(bf16[16,1024]{1,0:T(8,128)(2,1)S(1)} %get-tuple-element.40), channel_id=1, source_target_pairs={{0,8},{8,0},{16,24},{24,16},{1,9},{9,1},{17,25},{25,17},{2,10},{10... | collective-permute-start | bytes 98312 | tf_op jit(solution)/shard_map/ppermute | solution.py:37
  47.1 8.5 %collective-permute-start.19 = (bf16[16,1024]{1,0:T(8,128)(2,1)S(1)}, bf16[16,1024]{1,0:T(8,128)(2,1)S(1)}, u32[]{:S(2)}, u32[]{:S(2)}) collective-permute-start(bf16[16,1024]{1,0:T(8,128)(2,1)S(1)} %get-tuple-element.42), channel_id=1, source_target_pairs={{0,16},{8,24},{16,0},{24,8},{1,17},{9,25},{17,1},{25,9},{2,18},{10... | collective-permute-start | bytes 98312 | tf_op jit(solution)/shard_map/ppermute | solution.py:37
  48.0 7.6 %collective-permute-start.20 = (bf16[16,1024]{1,0:T(8,128)(2,1)S(1)}, bf16[16,1024]{1,0:T(8,128)(2,1)S(1)}, u32[]{:S(2)}, u32[]{:S(2)}) collective-permute-start(bf16[16,1024]{1,0:T(8,128)(2,1)S(1)} %get-tuple-element.41), channel_id=1, source_target_pairs={{0,24},{8,16},{16,8},{24,0},{1,25},{9,17},{17,9},{25,1},{2,26},{10... | collective-permute-start | bytes 98312 | tf_op jit(solution)/shard_map/ppermute | solution.py:37
where the time goes:
time: 56.5 us; the launch traced here: 56.4 us
  starting transfers between devices  20.6 us (36%)
  waiting for transfers between devices  18.6 us (33%)
  Pallas kernels  15.3 us (27%)
  other arithmetic  0.93 us (2%)
  between operations  0.82 us (1%)
    ppermute x21, starting transfers between devices, swap(): return lax.ppermute(value, axes, [(i, i ^ offset) for i in range(size)])  20.6 us
    ppermute x21, waiting for transfers between devices, swap(): return lax.ppermute(value, axes, [(i, i ^ offset) for i in range(size)])  18.6 us
    pallas_call x1, Pallas kernels, mixer(): pl.pallas_call(functools.partial(mixer_kernel, lanes), out_shape=(pltpu.V...  5.97 us
    pallas_call x1, Pallas kernels, update(): pl.pallas_call(update_kernel, out_shape=pltpu.HBM(state.shape, state.dtyp...  4.1 us
    pallas_call x1, Pallas kernels, fetch(): pl.pallas_call(functools.partial(fetch_kernel, len(arrays)), out_shape=[p...  2.88 us
    pallas_call x1, Pallas kernels, expert_slice(): pl.pallas_call(functools.partial(expert_kernel, mid, lanes), out_shape=[p...  2.33 us
  transfers between devices with their start and end apart: 21, of which 9 were waited for; matrix products, arithmetic and copies ran while one was open for 0% of the time, Pallas kernels for 12%

commit v1 on v0

--- a/solution.py
+++ b/solution.py
@@ -1,4 +1,5 @@
 import functools
+import itertools
 
 import jax
 import jax.numpy as jnp
@@ -13,7 +14,7 @@
 CORES = 2
 FILL_FLOPS = 1 << 30
 EP = ("outer", "mid", "core")
-PLANE = ("mid", "tp")
+PLANE = ("mid", "core", "tp")
 
 
 def rms_scale(values, gain):
@@ -39,6 +40,20 @@
 
 def columns(value, index, width):
     return lax.dynamic_slice_in_dim(value, index * width, width, 1)
+
+
+def turned(slot, lanes):
+    return {1: lanes, lanes: 1}.get(slot, slot)
+
+
+def plane_swap(value, slot):
+    mid, cores, lanes = map(lax.axis_size, PLANE)
+    pairs = []
+    for m, c, t in itertools.product(range(mid), range(cores), range(lanes)):
+        offset = turned(slot, lanes) if c else slot
+        target = ((m ^ offset // lanes) * cores + c) * lanes + (t ^ offset % lanes)
+        pairs.append(((m * cores + c) * lanes + t, target))
+    return lax.ppermute(value, PLANE, pairs)
 
 
 def split_two(value):
@@ -296,28 +311,44 @@
     def columns_of(offset):
         return pl.ds(pl.multiple_of((lane_index ^ offset) * width, width), width)
 
+    first_core = lax.axis_index("core") == 0
+
+    def of_core(values, slot, mirrored):
+        other = turned(slot, lanes)
+        if other == slot:
+            return values[slot][...]
+        pair = (values[other], values[slot]) if mirrored else (values[slot], values[other])
+        return jnp.where(first_core, pair[0][...], pair[1][...])
+
     for block in range(CORES * mid):
         rows = slice(block * band, (block + 1) * band)
-        parts = arrived[block * lanes : (block + 1) * lanes]
+        group, row_offset = divmod(block, mid)
+        held = arrived[group * pieces : (group + 1) * pieces]
+        parts = [of_core(held, row_offset * lanes + place, group == 1) for place in range(lanes)]
         squares = 0.0
         for part in parts:
-            value = part[...].astype(f32)
+            value = part.astype(f32)
             squares = squares + jnp.sum(value * value, axis=-1, keepdims=True)
         scale = lax.rsqrt(squares / model_width + EPS)
         for offset, part in enumerate(parts):
             where = columns_of(offset)
-            ffn_vmem[rows, where] = (part[...].astype(f32) * scale * gain_ref[:, where]).astype(
-                bf16
-            )
+            ffn_vmem[rows, where] = (part.astype(f32) * scale * gain_ref[:, where]).astype(bf16)
     ffn_in = ffn_vmem[...]
     gated = jnp.dot(ffn_in, gate_ref[0], preferred_element_type=f32)
     lifted = jnp.dot(ffn_in, up_ref[0], preferred_element_type=f32)
     hidden = (jax.nn.silu(gated) * lifted).astype(bf16)
-    for offset in range(lanes):
-        terms = jnp.dot(hidden, down_ref[0, :, columns_of(offset)], preferred_element_type=f32)
-        for block in range(CORES * mid):
-            out = outs[block * lanes + offset]
-            out[...] = terms[block * band : (block + 1) * band].astype(out.dtype)
+    terms = [
+        jnp.dot(hidden, down_ref[0, :, columns_of(offset)], preferred_element_type=f32)
+        for offset in range(lanes)
+    ]
+    for group in range(CORES):
+        values = [
+            terms[slot % lanes][(group * mid + slot // lanes) * band :][:band]
+            for slot in range(pieces)
+        ]
+        for slot in range(pieces):
+            out = outs[group * pieces + slot]
+            out[...] = of_core(values, slot, group == 1).astype(out.dtype)
 
 
 def expert_slice(arrived, ffn_gain, expert_gate, expert_up, expert_down):
@@ -402,15 +433,16 @@
     held = jnp.concatenate(
         [held] + [swap(held, "outer", offset) for offset in range(1, outer)], axis=0
     )
-    arrived = [held] + [swap(held, PLANE, offset) for offset in range(1, mid * lanes)]
+    arrived = [held] + [plane_swap(held, offset) for offset in range(1, mid * lanes)]
     arrived = arrived + [swap(piece, "core", 1) for piece in arrived]
-    fetched = fetch(sent, expert_gate, expert_up, expert_down)
+    fetched = fetch(sent, expert_gate, expert_up)
+    fetched += fetch(sent, expert_down)
     terms = expert_slice(arrived, ffn_gain, *fetched)
     own, other = terms[: mid * lanes], terms[mid * lanes :]
     total = own[0] + swap(other[0], "core", 1).astype(f32)
     for offset in range(1, mid * lanes):
         piece = (own[offset] + swap(other[offset], "core", 1).astype(f32)).astype(bf16)
-        total = total + swap(piece, PLANE, offset).astype(f32)
+        total = total + plane_swap(piece, offset).astype(f32)
     pieces = total.astype(bf16)
     moe = total[:rows] * weight_of(0)
     for offset in range(1, outer):

time: 56.5 us -> 57.1 us (1.011)
  Pallas kernels: 15.3 us -> 16.3 us
    ppermute x21 -> x15, waiting for transfers between devices: 18.6 us -> 8.03 us  [swap(): return lax.ppermute(value, axes, [(i, i ^ offset) for i in range(size)])]
    ppermute x0 -> x6, waiting for transfers between devices: none -> 10.2 us  [plane_swap(): return lax.ppermute(value, PLANE, pairs)]
    ppermute x21 -> x15, starting transfers between devices: 20.6 us -> 13.4 us  [swap(): return lax.ppermute(value, axes, [(i, i ^ offset) for i in range(size)])]
    ppermute x0 -> x6, starting transfers between devices: none -> 7.24 us  [plane_swap(): return lax.ppermute(value, PLANE, pairs)]
    pallas_call x1 -> x2, Pallas kernels: 2.88 us -> 3.84 us  [fetch(): pl.pallas_call(functools.partial(fetch_kernel, len(arrays)), out_shape=[p...]
  transfers between devices with their start and end apart: 21 -> 21, of which waited for: 9 -> 10; matrix products, arithmetic and copies ran while one was open for 0% -> 0% of each run, Pallas kernels for 12% -> 14%
where the time goes in v1:
time: 57.1 us; the launch traced here: 56.9 us
  starting transfers between devices  20.6 us (36%)
  waiting for transfers between devices  18.2 us (32%)
  Pallas kernels  16.3 us (29%)
  other arithmetic  0.93 us (2%)
  between operations  0.83 us (1%)
    ppermute x15, starting transfers between devices, swap(): return lax.ppermute(value, axes, [(i, i ^ offset) for i in range(size)])  13.4 us
    ppermute x6, waiting for transfers between devices, plane_swap(): return lax.ppermute(value, PLANE, pairs)  10.2 us
    ppermute x15, waiting for transfers between devices, swap(): return lax.ppermute(value, axes, [(i, i ^ offset) for i in range(size)])  8.03 us
    ppermute x6, starting transfers between devices, plane_swap(): return lax.ppermute(value, PLANE, pairs)  7.24 us
    pallas_call x1, Pallas kernels, mixer(): pl.pallas_call(functools.partial(mixer_kernel, lanes), out_shape=(pltpu.V...  5.97 us
    pallas_call x1, Pallas kernels, update(): pl.pallas_call(update_kernel, out_shape=pltpu.HBM(state.shape, state.dtyp...  4.1 us
    pallas_call x2, Pallas kernels, fetch(): pl.pallas_call(functools.partial(fetch_kernel, len(arrays)), out_shape=[p...  3.84 us
    pallas_call x1, Pallas kernels, expert_slice(): pl.pallas_call(functools.partial(expert_kernel, mid, lanes), out_shape=[p...  2.34 us
  transfers between devices with their start and end apart: 21, of which 10 were waited for; matrix products, arithmetic and copies ran while one was open for 0% of the time, Pallas kernels for 14%

profile of v1, /device:TPU:0, one launch (start us, length us, event | category | flops | bytes accessed | tf_op | source)
XLA Modules:
  0.0 56.9 jit_solution(6602450783848272581)
XLA Ops:
  0.6 6.0 %mixer.1 = (f32[16,1024]{1,0:T(8,128)S(1)}, bf16[16,1024]{1,0:T(8,128)(2,1)S(1)}, f32[16,512]{1,0:T(8,128)S(1)}, f32[16,512]{1,0:T(8,128)S(1)}, f32[16,4]{1,0:T(8,128)S(1)}) custom-call(bf16[16,2048]{1,0:T(8,128)(2,1)} %refs_0_.1, f32[1,2048]{1,0:T(1,128)} %bitcast.9, bf16[8,2048]{1,0:T(8,128)(2,1)} %bitcast.7, bf16[8,2048]{1,0:T(8,128)(2,1)} %bitcast.8, ...), custom_call_target="tpu_custom_call" | custom-call | tf_op jit(solution)/shard_map/mixer/pallas_call | solution.py:198
  6.6 3.0 %collective-permute-start = (bf16[16,1024]{1,0:T(8,128)(2,1)S(1)}, bf16[16,1024]{1,0:T(8,128)(2,1)S(1)}, u32[]{:S(2)}, u32[]{:S(2)}) collective-permute-start(bf16[16,1024]{1,0:T(8,128)(2,1)S(1)} %get-tuple-element.18.refs_0_), channel_id=1, source_target_pairs={{0,1},{1,0},{2,3},{3,2},{4,5},{5,4},{6,7},{7,6},{8,9},{9,8},{10,11... | collective-permute-start | bytes 98312 | tf_op jit(solution)/shard_map/ppermute | solution.py:38
  9.7 1.9 %collective-permute-done = bf16[16,1024]{1,0:T(8,128)(2,1)S(1)} collective-permute-done((bf16[16,1024]{1,0:T(8,128)(2,1)S(1)}, bf16[16,1024]{1,0:T(8,128)(2,1)S(1)}, u32[]{:S(2)}, u32[]{:S(2)}) %collective-permute-start) | collective-permute-done | bytes 32800 | tf_op jit(solution)/shard_map/ppermute | solution.py:38
  11.6 2.2 %collective-permute-start.1 = (bf16[16,1024]{1,0:T(8,128)(2,1)S(1)}, bf16[16,1024]{1,0:T(8,128)(2,1)S(1)}, u32[]{:S(2)}, u32[]{:S(2)}) collective-permute-start(bf16[16,1024]{1,0:T(8,128)(2,1)S(1)} %add_convert_fusion.3), channel_id=1, source_target_pairs={{0,8},{8,0},{16,24},{24,16},{1,9},{9,1},{17,25},{25,17},{2,10},{10... | collective-permute-start | bytes 98312 | tf_op jit(solution)/shard_map/ppermute | solution.py:38
  13.7 2.6 %collective-permute-start.2 = (bf16[16,1024]{1,0:T(8,128)(2,1)S(1)}, bf16[16,1024]{1,0:T(8,128)(2,1)S(1)}, u32[]{:S(2)}, u32[]{:S(2)}) collective-permute-start(bf16[16,1024]{1,0:T(8,128)(2,1)S(1)} %add_convert_fusion.3), channel_id=1, source_target_pairs={{0,16},{8,24},{16,0},{24,8},{1,17},{9,25},{17,1},{25,9},{2,18},{10... | collective-permute-start | bytes 98312 | tf_op jit(solution)/shard_map/ppermute | solution.py:38
  16.3 0.0 collective-permute-start.3
  16.3 0.0 collective-permute-done.1
  16.3 2.5 %collective-permute-done.2 = bf16[16,1024]{1,0:T(8,128)(2,1)S(1)} collective-permute-done((bf16[16,1024]{1,0:T(8,128)(2,1)S(1)}, bf16[16,1024]{1,0:T(8,128)(2,1)S(1)}, u32[]{:S(2)}, u32[]{:S(2)}) %collective-permute-start.2) | collective-permute-done | bytes 32800 | tf_op jit(solution)/shard_map/ppermute | solution.py:38
  18.8 3.2 %collective-permute-done.3 = bf16[16,1024]{1,0:T(8,128)(2,1)S(1)} collective-permute-done((bf16[16,1024]{1,0:T(8,128)(2,1)S(1)}, bf16[16,1024]{1,0:T(8,128)(2,1)S(1)}, u32[]{:S(2)}, u32[]{:S(2)}) %collective-permute-start.3) | collective-permute-done | bytes 32800 | tf_op jit(solution)/shard_map/ppermute | solution.py:38
  22.1 2.5 %collective-permute-start.6 = (bf16[64,1024]{1,0:T(8,128)(2,1)S(1)}, bf16[64,1024]{1,0:T(8,128)(2,1)S(1)}, u32[]{:S(2)}, u32[]{:S(2)}) collective-permute-start(bf16[64,1024]{1,0:T(8,128)(2,1)S(1)} %pad_maximum_fusion.refs_0_), channel_id=1, source_target_pairs={{0,5},{1,4},{2,7},{3,6},{4,1},{5,0},{6,3},{7,2},{8,13},{9,12},{10,... | collective-permute-start | bytes 393224 | tf_op jit(solution)/shard_map/ppermute | solution.py:56
  24.6 0.5 collective-permute-start.4
  25.1 0.5 collective-permute-start.5
  25.6 0.0 collective-permute-start.7
  25.6 2.4 %collective-permute-done.6.refs_3_ = bf16[64,1024]{1,0:T(8,128)(2,1)S(1)} collective-permute-done((bf16[64,1024]{1,0:T(8,128)(2,1)S(1)}, bf16[64,1024]{1,0:T(8,128)(2,1)S(1)}, u32[]{:S(2)}, u32[]{:S(2)}) %collective-permute-start.6) | collective-permute-done | bytes 131104 | tf_op jit(solution)/shard_map/ppermute | solution.py:56
  28.0 0.0 collective-permute-start.10
  28.0 1.5 %collective-permute-done.4.refs_1_ = bf16[64,1024]{1,0:T(8,128)(2,1)S(1)} collective-permute-done((bf16[64,1024]{1,0:T(8,128)(2,1)S(1)}, bf16[64,1024]{1,0:T(8,128)(2,1)S(1)}, u32[]{:S(2)}, u32[]{:S(2)}) %collective-permute-start.4) | collective-permute-done | bytes 131104 | tf_op jit(solution)/shard_map/ppermute | solution.py:56
  29.5 0.0 collective-permute-start.8
  29.5 0.5 collective-permute-done.5.refs_2_
  30.1 1.6 %fetch.3.refs_11_ = bf16[1,512,2048]{2,1,0:T(8,128)(2,1)S(1)} custom-call(bf16[16,1024]{1,0:T(8,128)(2,1)S(1)} %get-tuple-element.18.refs_0_, bf16[1,512,2048]{2,1,0:T(8,128)(2,1)} %refs_1_.3), custom_call_target="tpu_custom_call" | custom-call | flops 1073741824 | bytes 4194304 | tf_op jit(solution)/shard_map/fetch/pallas_call | solution.py:284
  31.7 0.0 copy-start
  31.7 2.2 %fetch.2 = (bf16[1,2048,512]{2,1,0:T(8,128)(2,1)S(1)}, bf16[1,2048,512]{2,1,0:T(8,128)(2,1)S(1)}) custom-call(bf16[16,1024]{1,0:T(8,128)(2,1)S(1)} %get-tuple-element.18.refs_0_, bf16[1,2048,512]{2,1,0:T(8,128)(2,1)} %refs_1_.2, bf16[1,2048,512]{2,1,0:T(8,128)(2,1)} %refs_2_.1), custom_call_target="tpu_custom_call" | custom-call | flops 1073741824 | bytes 8388608 | tf_op jit(solution)/shard_map/fetch/pallas_call | solution.py:284
  34.0 0.0 collective-permute-done.7.refs_4_
  34.0 0.0 collective-permute-done.10.refs_7_
  34.0 0.0 collective-permute-done.9.refs_6_
  34.0 0.0 copy-start.2
  34.0 0.0 copy-start.3
  34.0 2.3 %experts.1 = (f32[64,1024]{1,0:T(8,128)S(1)}, f32[64,1024]{1,0:T(8,128)S(1)}, f32[64,1024]{1,0:T(8,128)S(1)}, f32[64,1024]{1,0:T(8,128)S(1)}, bf16[64,1024]{1,0:...) custom-call(bf16[64,1024]{1,0:T(8,128)(2,1)S(1)} %pad_maximum_fusion.ref, ...), custom_call_target="tpu_custom_call" | custom-call | tf_op jit(solution)/shard_map/experts/pallas_call | solution.py:363
  36.4 0.6 %collective-permute-start.12 = (bf16[64,1024]{1,0:T(8,128)(2,1)S(1)}, bf16[64,1024]{1,0:T(8,128)(2,1)S(1)}, u32[]{:S(2)}, u32[]{:S(2)}) collective-permute-start(bf16[64,1024]{1,0:T(8,128)(2,1)S(1)} %get-tuple-element.24), channel_id=1, source_target_pairs={{0,2},{2,0},{1,3},{3,1},{4,6},{6,4},{5,7},{7,5},{8,10},{10,8},{9,1... | collective-permute-start | bytes 393224 | tf_op jit(solution)/shard_map/ppermute | solution.py:38
  37.0 0.1 collective-permute-start.14
  37.0 0.4 collective-permute-start.16
  37.5 0.1 collective-permute-start.11
  37.5 0.4 collective-permute-done.12
  38.0 1.6 %collective-permute-start.13 = (bf16[64,1024]{1,0:T(8,128)(2,1)S(1)}, bf16[64,1024]{1,0:T(8,128)(2,1)S(1)}, u32[]{:S(2)}, u32[]{:S(2)}) collective-permute-start(bf16[64,1024]{1,0:T(8,128)(2,1)S(1)} %add_convert_fusion.2), channel_id=1, source_target_pairs={{0,1},{1,0},{2,6},{3,7},{4,5},{5,4},{6,2},{7,3},{8,9},{9,8},{10,14... | collective-permute-start | bytes 393224 | tf_op jit(solution)/shard_map/ppermute | solution.py:56
  39.5 0.0 collective-permute-done.14
  39.6 0.9 %collective-permute-start.15 = (bf16[64,1024]{1,0:T(8,128)(2,1)S(1)}, bf16[64,1024]{1,0:T(8,128)(2,1)S(1)}, u32[]{:S(2)}, u32[]{:S(2)}) collective-permute-start(bf16[64,1024]{1,0:T(8,128)(2,1)S(1)} %add_convert_fusion.1), channel_id=1, source_target_pairs={{0,4},{1,5},{2,3},{3,2},{4,0},{5,1},{6,7},{7,6},{8,12},{9,13},{10,... | collective-permute-start | bytes 393224 | tf_op jit(solution)/shard_map/ppermute | solution.py:56
  40.5 0.0 collective-permute-done.16
  40.5 1.2 %collective-permute-start.17 = (bf16[64,1024]{1,0:T(8,128)(2,1)S(1)}, bf16[64,1024]{1,0:T(8,128)(2,1)S(1)}, u32[]{:S(2)}, u32[]{:S(2)}) collective-permute-start(bf16[64,1024]{1,0:T(8,128)(2,1)S(1)} %add_convert_fusion), channel_id=1, source_target_pairs={{0,5},{1,4},{2,7},{3,6},{4,1},{5,0},{6,3},{7,2},{8,13},{9,12},{10,... | collective-permute-start | bytes 393224 | tf_op jit(solution)/shard_map/ppermute | solution.py:56
  41.8 2.6 %collective-permute-done.13 = bf16[64,1024]{1,0:T(8,128)(2,1)S(1)} collective-permute-done((bf16[64,1024]{1,0:T(8,128)(2,1)S(1)}, bf16[64,1024]{1,0:T(8,128)(2,1)S(1)}, u32[]{:S(2)}, u32[]{:S(2)}) %collective-permute-start.13) | collective-permute-done | bytes 131104 | tf_op jit(solution)/shard_map/ppermute | solution.py:56
  44.4 0.2 collective-permute-done.15
  44.6 2.9 %collective-permute-done.17 = bf16[64,1024]{1,0:T(8,128)(2,1)S(1)} collective-permute-done((bf16[64,1024]{1,0:T(8,128)(2,1)S(1)}, bf16[64,1024]{1,0:T(8,128)(2,1)S(1)}, u32[]{:S(2)}, u32[]{:S(2)}) %collective-permute-start.17) | collective-permute-done | bytes 131104 | tf_op jit(solution)/shard_map/ppermute | solution.py:56
  47.5 0.1 fusion.9
  47.6 0.1 collective-permute-start.18
  47.7 0.9 %collective-permute-start.19 = (bf16[16,1024]{1,0:T(8,128)(2,1)S(1)}, bf16[16,1024]{1,0:T(8,128)(2,1)S(1)}, u32[]{:S(2)}, u32[]{:S(2)}) collective-permute-start(bf16[16,1024]{1,0:T(8,128)(2,1)S(1)} %get-tuple-element.40), channel_id=1, source_target_pairs={{0,16},{8,24},{16,0},{24,8},{1,17},{9,25},{17,1},{25,9},{2,18},{10... | collective-permute-start | bytes 98312 | tf_op jit(solution)/shard_map/ppermute | solution.py:38
  48.6 3.5 %collective-permute-start.20 = (bf16[16,1024]{1,0:T(8,128)(2,1)S(1)}, bf16[16,1024]{1,0:T(8,128)(2,1)S(1)}, u32[]{:S(2)}, u32[]{:S(2)}) collective-permute-start(bf16[16,1024]{1,0:T(8,128)(2,1)S(1)} %get-tuple-element.39), channel_id=1, source_target_pairs={{0,24},{8,16},{16,8},{24,0},{1,25},{9,17},{17,9},{25,1},{2,26},{10... | collective-permute-start | bytes 98312 | tf_op jit(solution)/shard_map/ppermute | solution.py:38
  52.1 4.1 %update.1 = f32[16,4,128,128]{3,2,1,0:T(8,128)} custom-call(f32[16,4,128,128]{3,2,1,0:T(8,128)} %state_hbm.1, f32[16,512]{1,0:T(8,128)S(1)} %get-tuple-element.29.key_ref, f32[16,512]{1,0:T(8,128)S(1)} %get-tuple-element.30.written_ref, f32[16,4]{1,0:T(8,128)S(1)} %get-tuple-element.31.fade_ref), custom_call_target="tpu_custom_call" | custom-call | flops 1073741824 | bytes 8388608 | tf_op jit(solution)/shard_map/update/pallas_call | solution.py:254
  56.2 0.0 collective-permute-done.18
  56.2 0.0 collective-permute-done.19
  56.2 0.7 %fusion.4 = bf16[16,1024]{1,0:T(8,128)(2,1)} fusion(f32[64,1024]{1,0:T(8,128)S(1)} %get-tuple-element.37, bf16[16,1024]{1,0:T(8,128)(2,1)S(1)} %collective-permute-done.20, bf16[16,1024]{1,0:T(8,128)(2,1)S(1)} %collective-permute-done.19, bf16[16,1024]{1,0:T(8,128)(2,1)S(1)} %collective-permute-done.18, bf16[16,1024]{1,0:T(8,128)(2,1)S(1)} %add_convert_fusion.3, ...), kind=kLoop, calls=%fused_computation.10 | loop fusion | flops 212992 | bytes 229632 | tf_op jit(solution)/shard_map/convert_element_type | solution.py:451
  (16 shorter events, 0.2 us)
Async XLA Ops:
  0.6 10.9 %copy-start.1 = (bf16[16,2048]{1,0:T(8,128)(2,1)S(1)}, bf16[16,2048]{1,0:T(8,128)(2,1)}, u32[]{:S(2)}) copy-start(bf16[16,2048]{1,0:T(8,128)(2,1)} %refs_0_.1) | copy-start | bytes 196612
  6.6 4.9 %collective-permute-start = (bf16[16,1024]{1,0:T(8,128)(2,1)S(1)}, bf16[16,1024]{1,0:T(8,128)(2,1)S(1)}, u32[]{:S(2)}, u32[]{:S(2)}) collective-permute-start(bf16[16,1024]{1,0:T(8,128)(2,1)S(1)} %get-tuple-element.18.refs_0_), channel_id=1, source_target_pairs={{0,1},{1,0},{2,3},{3,2},{4,5},{5,4},{6,7},{7,6},{8,9},{9,8},{10,11... | collective-permute-start | bytes 98312 | tf_op jit(solution)/shard_map/ppermute | solution.py:38
  11.6 4.8 %collective-permute-start.1 = (bf16[16,1024]{1,0:T(8,128)(2,1)S(1)}, bf16[16,1024]{1,0:T(8,128)(2,1)S(1)}, u32[]{:S(2)}, u32[]{:S(2)}) collective-permute-start(bf16[16,1024]{1,0:T(8,128)(2,1)S(1)} %add_convert_fusion.3), channel_id=1, source_target_pairs={{0,8},{8,0},{16,24},{24,16},{1,9},{9,1},{17,25},{25,17},{2,10},{10... | collective-permute-start | bytes 98312 | tf_op jit(solution)/shard_map/ppermute | solution.py:38
  13.7 5.1 %collective-permute-start.2 = (bf16[16,1024]{1,0:T(8,128)(2,1)S(1)}, bf16[16,1024]{1,0:T(8,128)(2,1)S(1)}, u32[]{:S(2)}, u32[]{:S(2)}) collective-permute-start(bf16[16,1024]{1,0:T(8,128)(2,1)S(1)} %add_convert_fusion.3), channel_id=1, source_target_pairs={{0,16},{8,24},{16,0},{24,8},{1,17},{9,25},{17,1},{25,9},{2,18},{10... | collective-permute-start | bytes 98312 | tf_op jit(solution)/shard_map/ppermute | solution.py:38
  16.3 5.7 %collective-permute-start.3 = (bf16[16,1024]{1,0:T(8,128)(2,1)S(1)}, bf16[16,1024]{1,0:T(8,128)(2,1)S(1)}, u32[]{:S(2)}, u32[]{:S(2)}) collective-permute-start(bf16[16,1024]{1,0:T(8,128)(2,1)S(1)} %add_convert_fusion.3), channel_id=1, source_target_pairs={{0,24},{8,16},{16,8},{24,0},{1,25},{9,17},{17,9},{25,1},{2,26},{10... | collective-permute-start | bytes 98312 | tf_op jit(solution)/shard_map/ppermute | solution.py:38
  22.1 5.9 %collective-permute-start.6 = (bf16[64,1024]{1,0:T(8,128)(2,1)S(1)}, bf16[64,1024]{1,0:T(8,128)(2,1)S(1)}, u32[]{:S(2)}, u32[]{:S(2)}) collective-permute-start(bf16[64,1024]{1,0:T(8,128)(2,1)S(1)} %pad_maximum_fusion.refs_0_), channel_id=1, source_target_pairs={{0,5},{1,4},{2,7},{3,6},{4,1},{5,0},{6,3},{7,2},{8,13},{9,12},{10,... | collective-permute-start | bytes 393224 | tf_op jit(solution)/shard_map/ppermute | solution.py:56
  24.6 5.0 %collective-permute-start.4 = (bf16[64,1024]{1,0:T(8,128)(2,1)S(1)}, bf16[64,1024]{1,0:T(8,128)(2,1)S(1)}, u32[]{:S(2)}, u32[]{:S(2)}) collective-permute-start(bf16[64,1024]{1,0:T(8,128)(2,1)S(1)} %pad_maximum_fusion.refs_0_), channel_id=1, source_target_pairs={{0,1},{1,0},{2,6},{3,7},{4,5},{5,4},{6,2},{7,3},{8,9},{9,8},{10,14... | collective-permute-start | bytes 393224 | tf_op jit(solution)/shard_map/ppermute | solution.py:56
  25.1 5.0 %collective-permute-start.5 = (bf16[64,1024]{1,0:T(8,128)(2,1)S(1)}, bf16[64,1024]{1,0:T(8,128)(2,1)S(1)}, u32[]{:S(2)}, u32[]{:S(2)}) collective-permute-start(bf16[64,1024]{1,0:T(8,128)(2,1)S(1)} %pad_maximum_fusion.refs_0_), channel_id=1, source_target_pairs={{0,4},{1,5},{2,3},{3,2},{4,0},{5,1},{6,7},{7,6},{8,12},{9,13},{10,... | collective-permute-start | bytes 393224 | tf_op jit(solution)/shard_map/ppermute | solution.py:56
  25.6 8.3 %collective-permute-start.7 = (bf16[64,1024]{1,0:T(8,128)(2,1)S(1)}, bf16[64,1024]{1,0:T(8,128)(2,1)S(1)}, u32[]{:S(2)}, u32[]{:S(2)}) collective-permute-start(bf16[64,1024]{1,0:T(8,128)(2,1)S(1)} %pad_maximum_fusion.refs_0_), channel_id=1, source_target_pairs={{0,2},{2,0},{1,3},{3,1},{4,6},{6,4},{5,7},{7,5},{8,10},{10,8},{9,1... | collective-permute-start | bytes 393224 | tf_op jit(solution)/shard_map/ppermute | solution.py:38
  28.0 6.0 %collective-permute-start.10 = (bf16[64,1024]{1,0:T(8,128)(2,1)S(1)}, bf16[64,1024]{1,0:T(8,128)(2,1)S(1)}, u32[]{:S(2)}, u32[]{:S(2)}) collective-permute-start(bf16[64,1024]{1,0:T(8,128)(2,1)S(1)} %collective-permute-done.6.refs_3_), channel_id=1, source_target_pairs={{0,2},{2,0},{1,3},{3,1},{4,6},{6,4},{5,7},{7,5},{8,10},{10,8},{9,1... | collective-permute-start | bytes 393224 | tf_op jit(solution)/shard_map/ppermute | solution.py:38
  29.5 4.4 %collective-permute-start.8 = (bf16[64,1024]{1,0:T(8,128)(2,1)S(1)}, bf16[64,1024]{1,0:T(8,128)(2,1)S(1)}, u32[]{:S(2)}, u32[]{:S(2)}) collective-permute-start(bf16[64,1024]{1,0:T(8,128)(2,1)S(1)} %collective-permute-done.4.refs_1_), channel_id=1, source_target_pairs={{0,2},{2,0},{1,3},{3,1},{4,6},{6,4},{5,7},{7,5},{8,10},{10,8},{9,1... | collective-permute-start | bytes 393224 | tf_op jit(solution)/shard_map/ppermute | solution.py:38
  30.1 3.9 %collective-permute-start.9 = (bf16[64,1024]{1,0:T(8,128)(2,1)S(1)}, bf16[64,1024]{1,0:T(8,128)(2,1)S(1)}, u32[]{:S(2)}, u32[]{:S(2)}) collective-permute-start(bf16[64,1024]{1,0:T(8,128)(2,1)S(1)} %collective-permute-done.5.refs_2_), channel_id=1, source_target_pairs={{0,2},{2,0},{1,3},{3,1},{4,6},{6,4},{5,7},{7,5},{8,10},{10,8},{9,1... | collective-permute-start | bytes 393224 | tf_op jit(solution)/shard_map/ppermute | solution.py:38
  31.7 2.3 %copy-start = (f32[2048]{0:T(1024)S(1)}, f32[2048]{0:T(1024)}, u32[]{:S(2)}) copy-start(f32[2048]{0:T(1024)} %param.30) | copy-start | bytes 24580
  34.0 7.7 %copy-start.2 = (f32[16,2]{0,1:T(2,128)S(1)}, f32[16,2]{0,1:T(2,128)}, u32[]{:S(2)}) copy-start(f32[16,2]{0,1:T(2,128)} %param.32) | copy-start | bytes 388
  34.0 7.7 %copy-start.3 = (s32[16,2]{0,1:T(2,128)S(1)}, s32[16,2]{0,1:T(2,128)}, u32[]{:S(2)}) copy-start(s32[16,2]{0,1:T(2,128)} %param.31) | copy-start | bytes 388
  36.4 1.6 %collective-permute-start.12 = (bf16[64,1024]{1,0:T(8,128)(2,1)S(1)}, bf16[64,1024]{1,0:T(8,128)(2,1)S(1)}, u32[]{:S(2)}, u32[]{:S(2)}) collective-permute-start(bf16[64,1024]{1,0:T(8,128)(2,1)S(1)} %get-tuple-element.24), channel_id=1, source_target_pairs={{0,2},{2,0},{1,3},{3,1},{4,6},{6,4},{5,7},{7,5},{8,10},{10,8},{9,1... | collective-permute-start | bytes 393224 | tf_op jit(solution)/shard_map/ppermute | solution.py:38
  37.0 2.6 %collective-permute-start.14 = (bf16[64,1024]{1,0:T(8,128)(2,1)S(1)}, bf16[64,1024]{1,0:T(8,128)(2,1)S(1)}, u32[]{:S(2)}, u32[]{:S(2)}) collective-permute-start(bf16[64,1024]{1,0:T(8,128)(2,1)S(1)} %get-tuple-element.26), channel_id=1, source_target_pairs={{0,2},{2,0},{1,3},{3,1},{4,6},{6,4},{5,7},{7,5},{8,10},{10,8},{9,1... | collective-permute-start | bytes 393224 | tf_op jit(solution)/shard_map/ppermute | solution.py:38
  37.0 3.4 %collective-permute-start.16 = (bf16[64,1024]{1,0:T(8,128)(2,1)S(1)}, bf16[64,1024]{1,0:T(8,128)(2,1)S(1)}, u32[]{:S(2)}, u32[]{:S(2)}) collective-permute-start(bf16[64,1024]{1,0:T(8,128)(2,1)S(1)} %get-tuple-element.28), channel_id=1, source_target_pairs={{0,2},{2,0},{1,3},{3,1},{4,6},{6,4},{5,7},{7,5},{8,10},{10,8},{9,1... | collective-permute-start | bytes 393224 | tf_op jit(solution)/shard_map/ppermute | solution.py:38
  37.5 4.3 %collective-permute-start.11 = (bf16[64,1024]{1,0:T(8,128)(2,1)S(1)}, bf16[64,1024]{1,0:T(8,128)(2,1)S(1)}, u32[]{:S(2)}, u32[]{:S(2)}) collective-permute-start(bf16[64,1024]{1,0:T(8,128)(2,1)S(1)} %get-tuple-element.22), channel_id=1, source_target_pairs={{0,2},{2,0},{1,3},{3,1},{4,6},{6,4},{5,7},{7,5},{8,10},{10,8},{9,1... | collective-permute-start | bytes 393224 | tf_op jit(solution)/shard_map/ppermute | solution.py:38
  38.0 6.4 %collective-permute-start.13 = (bf16[64,1024]{1,0:T(8,128)(2,1)S(1)}, bf16[64,1024]{1,0:T(8,128)(2,1)S(1)}, u32[]{:S(2)}, u32[]{:S(2)}) collective-permute-start(bf16[64,1024]{1,0:T(8,128)(2,1)S(1)} %add_convert_fusion.2), channel_id=1, source_target_pairs={{0,1},{1,0},{2,6},{3,7},{4,5},{5,4},{6,2},{7,3},{8,9},{9,8},{10,14... | collective-permute-start | bytes 393224 | tf_op jit(solution)/shard_map/ppermute | solution.py:56
  39.6 5.0 %collective-permute-start.15 = (bf16[64,1024]{1,0:T(8,128)(2,1)S(1)}, bf16[64,1024]{1,0:T(8,128)(2,1)S(1)}, u32[]{:S(2)}, u32[]{:S(2)}) collective-permute-start(bf16[64,1024]{1,0:T(8,128)(2,1)S(1)} %add_convert_fusion.1), channel_id=1, source_target_pairs={{0,4},{1,5},{2,3},{3,2},{4,0},{5,1},{6,7},{7,6},{8,12},{9,13},{10,... | collective-permute-start | bytes 393224 | tf_op jit(solution)/shard_map/ppermute | solution.py:56
  40.5 7.0 %collective-permute-start.17 = (bf16[64,1024]{1,0:T(8,128)(2,1)S(1)}, bf16[64,1024]{1,0:T(8,128)(2,1)S(1)}, u32[]{:S(2)}, u32[]{:S(2)}) collective-permute-start(bf16[64,1024]{1,0:T(8,128)(2,1)S(1)} %add_convert_fusion), channel_id=1, source_target_pairs={{0,5},{1,4},{2,7},{3,6},{4,1},{5,0},{6,3},{7,2},{8,13},{9,12},{10,... | collective-permute-start | bytes 393224 | tf_op jit(solution)/shard_map/ppermute | solution.py:56
  47.6 8.6 %collective-permute-start.18 = (bf16[16,1024]{1,0:T(8,128)(2,1)S(1)}, bf16[16,1024]{1,0:T(8,128)(2,1)S(1)}, u32[]{:S(2)}, u32[]{:S(2)}) collective-permute-start(bf16[16,1024]{1,0:T(8,128)(2,1)S(1)} %get-tuple-element.38), channel_id=1, source_target_pairs={{0,8},{8,0},{16,24},{24,16},{1,9},{9,1},{17,25},{25,17},{2,10},{10... | collective-permute-start | bytes 98312 | tf_op jit(solution)/shard_map/ppermute | solution.py:38
  47.7 8.5 %collective-permute-start.19 = (bf16[16,1024]{1,0:T(8,128)(2,1)S(1)}, bf16[16,1024]{1,0:T(8,128)(2,1)S(1)}, u32[]{:S(2)}, u32[]{:S(2)}) collective-permute-start(bf16[16,1024]{1,0:T(8,128)(2,1)S(1)} %get-tuple-element.40), channel_id=1, source_target_pairs={{0,16},{8,24},{16,0},{24,8},{1,17},{9,25},{17,1},{25,9},{2,18},{10... | collective-permute-start | bytes 98312 | tf_op jit(solution)/shard_map/ppermute | solution.py:38
  48.6 7.6 %collective-permute-start.20 = (bf16[16,1024]{1,0:T(8,128)(2,1)S(1)}, bf16[16,1024]{1,0:T(8,128)(2,1)S(1)}, u32[]{:S(2)}, u32[]{:S(2)}) collective-permute-start(bf16[16,1024]{1,0:T(8,128)(2,1)S(1)} %get-tuple-element.39), channel_id=1, source_target_pairs={{0,24},{8,16},{16,8},{24,0},{1,25},{9,17},{17,9},{25,1},{2,26},{10... | collective-permute-start | bytes 98312 | tf_op jit(solution)/shard_map/ppermute | solution.py:38
